TPU v7x, 32 devices: a whole 2x2x4 slice. The times are simulated.
32 devices in a mesh: gr: 2 (over y), sp: 4 (over z), tp: 4 (over x, core).
Axes of the slice: x: 2, y: 2, z: 4, core: 2. Of those that a mesh axis runs over, the one named last changes fastest.
Arguments:
- tokens: bfloat16 [4, 1024, 4096], P('gr', ('sp', 'tp')), parts along dimension 0, may hold values from -6 to 6
- norm_gain: bfloat16 [4096], replicated, may hold values from 0.099609375 to 1.8984375
- key_weight: bfloat16 [4096, 1024], P(None, 'tp'), may hold values from -0.09375 to 0.09375
- value_weight: bfloat16 [4096, 1024], P(None, 'tp'), may hold values from -0.09375 to 0.09375
- cum_gates: float32 [4, 1024, 16], P('gr', 'sp', 'tp'), parts along dimension 0, may hold values from -173 to 0, as said below
- new_query: bfloat16 [4, 1024], P('gr', 'tp'), parts along dimension 0, may hold values from -240 to 240
- new_key: bfloat16 [4, 1024], P('gr', 'tp'), parts along dimension 0, may hold values from -6 to 6
- new_value: bfloat16 [4, 1024], P('gr', 'tp'), parts along dimension 0, may hold values from -6 to 6
- new_gate: float32 [4, 16], P('gr', 'tp'), parts along dimension 0, may hold values from -5 to -1.5
Outputs:
- key_cache: bfloat16 [4, 1024, 1024], P('gr', 'sp', 'tp'), parts along dimension 0
- value_cache: bfloat16 [4, 1024, 1024], P('gr', 'sp', 'tp'), parts along dimension 0
- readout: bfloat16 [4, 1024], P('gr', 'tp'), parts along dimension 0
There are 2 independent parts, one for each index of `gr`. A program takes and returns all parts, laid end to end along the dimension named above; an argument that names none is the same for every part. Nothing has to cross between parts.
Inputs may be any that keep to these rules, and one draw needn't show every extreme that they name: `cum_gates`: along positions, for each prompt and head, the values never rise.
All inputs are finite; a program needn't handle non-finite values.
Results may differ from a plain program's by a relative error of at most 0.005.
The roundings to bfloat16 on the way count: a program that leaves them out, or rounds other values in their place, can miss the bound.
Values may be sent and summed in bfloat16 or wider, within the bound.
A program may use at most 64 MiB of HBM per device.

v0:
```python
import jax
import jax.numpy as jnp
from jax import lax
from jax.sharding import PartitionSpec as P

HD = 64
epsilon = 1e-06
masked_score = -1e30


def body(
    tokens, norm_gain, key_weight, value_weight, cum_gates, new_query, new_key, new_value, new_gate
):
    seq_count, own_len, model_width = tokens.shape
    as_float = tokens.astype(jnp.float32)
    normed = (
        as_float
        * lax.rsqrt(jnp.mean(as_float * as_float, axis=-1, keepdims=True) + epsilon)
        * norm_gain.astype(jnp.float32)
    ).astype(jnp.bfloat16)
    key_width = key_weight.shape[1]
    local_heads = key_width // HD
    both_weights = jnp.concatenate([key_weight, value_weight], axis=1)
    piece = lax.all_gather(normed, "tp", axis=1, tiled=True)
    piece_len = piece.shape[1]
    rows = piece.reshape(seq_count * piece_len, model_width)
    result = jnp.dot(rows, both_weights, preferred_element_type=jnp.float32).astype(jnp.bfloat16)
    projected = result.reshape(seq_count, piece_len, 2 * key_width)
    key_cache = projected[:, :, :key_width]
    value_cache = projected[:, :, key_width:]
    block_len = projected.shape[1]
    sp_count = lax.axis_size("sp")
    sp_index = lax.axis_index("sp")
    score_scale = HD ** (-0.5)
    queries = new_query.reshape(seq_count, local_heads, HD)
    fresh_key = new_key.reshape(seq_count, local_heads, HD).astype(jnp.float32)
    fresh_value = new_value.reshape(seq_count, local_heads, HD).astype(jnp.float32)
    fresh_score = jnp.sum(queries.astype(jnp.float32) * fresh_key, axis=-1) * score_scale
    key_heads = key_cache.reshape(seq_count, block_len, local_heads, HD)
    value_heads = value_cache.reshape(seq_count, block_len, local_heads, HD).astype(jnp.float32)
    scores = (
        jnp.einsum("shd,slhd->shl", queries, key_heads, preferred_element_type=jnp.float32)
        * score_scale
    )
    scores = scores - jnp.transpose(cum_gates, (0, 2, 1))
    last_block = sp_index == sp_count - 1
    fresh_term = jnp.where(
        last_block, fresh_score - (cum_gates[:, block_len - 1, :] + new_gate), masked_score
    )
    local_top = jnp.maximum(jnp.max(scores, axis=-1), fresh_term)
    maxima = lax.pmax(local_top, "sp")
    weights = jnp.exp(scores - maxima[:, :, None])
    fresh_weight = jnp.exp(fresh_term - maxima)
    totals = jnp.sum(weights, axis=-1) + fresh_weight
    weighted = jnp.einsum("shl,slhd->shd", weights, value_heads, precision=lax.Precision.HIGHEST)
    weighted = weighted + fresh_weight[:, :, None] * fresh_value
    totals, weighted = lax.psum((totals, weighted), "sp")
    readout = (weighted / totals[:, :, None]).reshape(seq_count, key_width).astype(jnp.bfloat16)
    return (key_cache, value_cache, readout)


def solution(mesh):
    in_specs = (
        P("gr", ("sp", "tp"), None),
        P(),
        P(None, "tp"),
        P(None, "tp"),
        P("gr", "sp", "tp"),
        P("gr", "tp"),
        P("gr", "tp"),
        P("gr", "tp"),
        P("gr", "tp"),
    )
    out_specs = (P("gr", "sp", "tp"), P("gr", "sp", "tp"), P("gr", "tp"))
    return jax.shard_map(body, mesh=mesh, in_specs=in_specs, out_specs=out_specs, check_vma=False)
```

profile of v0, /device:TPU:0, one launch (start us, length us, event | category | flops | bytes accessed | tf_op | source)
XLA Modules:
  0.0 83.7 jit_solution(6548077247722289311)
XLA Ops:
  7.2 0.0 all-gather.2.cloned.1.call-start
  7.2 0.7 convert_element_type.35
  7.9 1.7 %fusion.4 = f32[2,64]{1,0:T(2,128)S(1)} fusion(bf16[2,64,4096]{2,1,0:T(8,128)(2,1)} %param.9), kind=kLoop, calls=%fused_computation.6 | loop fusion | flops 1572736 | bytes 1049088 | tf_op jit(solution)/shard_map/reduce_sum | solution.py:18
  9.6 2.5 %fusion.6 = bf16[2,64,4096]{2,1,0:T(8,128)(2,1)} fusion(bf16[2,64,4096]{2,1,0:T(8,128)(2,1)} %param.9, f32[4096]{0:T(1024)S(1)} %convert_element_type.35, f32[2,64]{1,0:T(2,128)S(1)} %add_rsqrt_fusion), kind=kLoop, calls=%fused_computation.8 | loop fusion | flops 2097152 | bytes 2114048 | tf_op jit(solution)/shard_map/convert_element_type | solution.py:20
  12.2 0.0 all-gather.2.cloned.1.call-update
  12.2 0.1 reshape.53
  12.3 0.1 reshape.44
  12.4 0.1 reshape.46
  12.4 0.1 reshape.47
  12.5 0.2 slice_reduce_fusion
  12.7 0.1 multiply_reduce_fusion
  12.8 36.7 %all-gather.2.cloned.1.call-done = bf16[2,256,4096]{2,1,0:T(8,128)(2,1)} async-done(((bf16[2,64,4096]{2,1,0:T(8,128)(2,1)}), bf16[2,256,4096]{2,1,0:T(8,128)(2,1)}) %all-gather.2.cloned.1.call-update) | async-done | bytes 4194320 | tf_op jit(solution)/shard_map/all_gather | solution.py:24
  49.5 5.2 %fusion.7 = bf16[512,512]{1,0:T(8,128)(2,1)S(1)} fusion(bf16[512,4096]{1,0:T(8,128)(2,1)} %bitcast.34, bf16[4096,256]{1,0:T(8,128)(2,1)S(1)} %copy-done.7, bf16[4096,256]{1,0:T(8,128)(2,1)} %param.11), kind=kOutput, calls=%fused_computation.9 | convolution fusion | flops 2156134400 | bytes 8912896 | tf_op jit(solution)/shard_map/dot_general | solution.py:27
  54.8 0.1 copy.20
  55.0 0.1 fusion.19
  55.1 0.1 fusion.15
  55.2 11.7 %pmax.7 = f32[2,4]{1,0:T(2,128)S(1)} all-reduce(f32[2,4]{1,0:T(2,128)S(1)} %get-tuple-element.10), channel_id=1, replica_groups=mesh['gr'=2,'sp'=4,'tp'=4] {'sp'}, use_global_device_ids=true, to_apply=%region_3.4 | all-reduce | flops 8 | bytes 64 | tf_op jit(solution)/shard_map/pmax | solution.py:51
  66.9 0.2 fusion.12
  67.1 0.1 copy.21
  67.2 0.3 fusion.10
  67.5 0.1 multiply_add_fusion
  67.6 8.5 %all-reduce = (f32[2,4,64]{2,1,0:T(4,128)S(1)}, f32[2,4]{1,0:T(2,128)S(1)}) all-reduce(f32[2,4,64]{2,1,0:T(4,128)S(1)} %multiply_add_fusion, f32[2,4]{1,0:T(2,128)S(1)} %get-tuple-element.8), channel_id=1, replica_groups=mesh['gr'=2,'sp'=4,'tp'=4] {'sp'}, use_global_device_ids=true, to_apply=%region_4.5 | all-reduce | flops 520 | bytes 4160 | tf_op jit(solution)/shard_map/psum | solution.py:57
  76.1 0.1 divide_convert_fusion
  76.2 0.7 convert_element_type.44
  (20 shorter events, 0.1 us)
Async XLA Ops:
  7.2 42.3 %all-gather.2.cloned.1.call-start = ((), (), s32[]{:S(2)}) async-start(), calls=%async_computation | async-start | bytes 5242880 | tf_op jit(solution)/shard_map/all_gather | solution.py:24
  7.9 4.3 %copy-start.3 = (bf16[2,256]{1,0:T(2,128)(2,1)S(1)}, bf16[2,256]{1,0:T(2,128)(2,1)}, u32[]{:S(2)}) copy-start(bf16[2,256]{1,0:T(2,128)(2,1)} %param.14) | copy-start | bytes 3076
  7.9 4.4 %copy-start.4 = (bf16[2,256]{1,0:T(2,128)(2,1)S(1)}, bf16[2,256]{1,0:T(2,128)(2,1)}, u32[]{:S(2)}) copy-start(bf16[2,256]{1,0:T(2,128)(2,1)} %param.15) | copy-start | bytes 3076
  7.9 4.5 %copy-start.5 = (bf16[2,256]{1,0:T(2,128)(2,1)S(1)}, bf16[2,256]{1,0:T(2,128)(2,1)}, u32[]{:S(2)}) copy-start(bf16[2,256]{1,0:T(2,128)(2,1)} %param.16) | copy-start | bytes 3076
  7.9 4.6 %copy-start.2 = (f32[2,256,4]{1,2,0:T(4,128)S(1)}, f32[2,256,4]{1,2,0:T(4,128)}, u32[]{:S(2)}) copy-start(f32[2,256,4]{1,2,0:T(4,128)} %param.13) | copy-start | bytes 24580
  7.9 41.6 %copy-start.7 = (bf16[4096,256]{1,0:T(8,128)(2,1)S(1)}, bf16[4096,256]{1,0:T(8,128)(2,1)}, u32[]{:S(2)}) copy-start(bf16[4096,256]{1,0:T(8,128)(2,1)} %param.12) | copy-start | bytes 6291460
  49.5 5.7 %copy-start.6 = (f32[2,4]{1,0:T(2,128)S(1)}, f32[2,4]{1,0:T(2,128)}, u32[]{:S(2)}) copy-start(f32[2,4]{1,0:T(2,128)} %param.17) | copy-start | bytes 100
  54.8 22.1 %copy-start = (bf16[2,256,256]{2,1,0:T(8,128)(2,1)}, bf16[2,256,256]{2,1,0:T(8,128)(2,1)S(1)}, u32[]{:S(2)}) copy-start(bf16[2,256,256]{2,1,0:T(8,128)(2,1)S(1)} %get-tuple-element.12) | copy-start | bytes 786436
  54.8 22.0 %copy-start.1 = (bf16[2,256,256]{2,1,0:T(8,128)(2,1)}, bf16[2,256,256]{2,1,0:T(8,128)(2,1)S(1)}, u32[]{:S(2)}) copy-start(bf16[2,256,256]{2,1,0:T(8,128)(2,1)S(1)} %get-tuple-element.13) | copy-start | bytes 786436
Sparse Core Ops, SparseCore 0:
  12.3 37.1 all-gather.1
where the time goes:
time: 84 us; the launch traced here: 83.7 us
  waiting for transfers between devices  36.8 us (44%)
  blocking collectives  20.2 us (24%)
  between operations  14.1 us (17%)
  matrix products  5.69 us (7%)
  other arithmetic  5.42 us (6%)
  local copies, waits for them, and re-layouts  1.48 us (2%)
    all_gather x1, waiting for transfers between devices, body(): piece = lax.all_gather(normed, 'tp', axis=1, tiled=True)  36.7 us
    pmax x1, blocking collectives, body(): maxima = lax.pmax(local_top, 'sp')  11.7 us
    psum x1, blocking collectives, body(): totals, weighted = lax.psum((totals, weighted), 'sp')  8.5 us
    dot_general x1, matrix products, body(): jnp.dot(rows, both_weights, preferred_element_type=jnp.float32)  5.24 us
    convert_element_type x1, other arithmetic, body(): normed = (as_float * lax.rsqrt(jnp.mean(as_float * as_float, axis=-1, kee...  2.53 us
  transfers between devices with their start and end apart: 1, of which 1 were waited for; matrix products, arithmetic and copies ran while one was open for 1% of the time, Pallas kernels for 0%

commit v1 on v0

--- a/solution.py
+++ b/solution.py
@@ -21,7 +21,12 @@
     key_width = key_weight.shape[1]
     local_heads = key_width // HD
     both_weights = jnp.concatenate([key_weight, value_weight], axis=1)
-    piece = lax.all_gather(normed, "tp", axis=1, tiled=True)
+    ring = [normed]
+    for hop in range(3):
+        ring.append(lax.ppermute(ring[-1], "tp", [(dev, (dev + 1) % 4) for dev in range(4)]))
+    piece = jnp.roll(
+        jnp.concatenate(ring[::-1], axis=1), (lax.axis_index("tp") + 1) * ring[0].shape[1], axis=1
+    )
     piece_len = piece.shape[1]
     rows = piece.reshape(seq_count * piece_len, model_width)
     result = jnp.dot(rows, both_weights, preferred_element_type=jnp.float32).astype(jnp.bfloat16)

time: 84 us -> 79.8 us (0.950)
  between operations: 14.1 us -> 0.8 us
  local copies, waits for them, and re-layouts: 1.48 us -> 9.94 us
  matrix products: 5.69 us -> 2.8 us
  waiting for transfers between devices: 36.8 us -> 39 us
  blocking collectives: 20.2 us -> 21.3 us
    ppermute x0 -> x3, waiting for transfers between devices: none -> 39 us  [body(): lax.ppermute(ring[-1], 'tp', [(dev, (dev + 1) % 4) for dev in range(4)])]
    all_gather x1 -> x0, waiting for transfers between devices: 36.7 us -> none  [body(): piece = lax.all_gather(normed, 'tp', axis=1, tiled=True)]
    unnamed x18 -> x22, local copies, waits for them, and re-layouts: 0.3 us -> 4.87 us
    dot_general x1, matrix products: 5.24 us -> 2.35 us  [body(): jnp.dot(rows, both_weights, preferred_element_type=jnp.float32)]
    reshape x2, local copies, waits for them, and re-layouts: 0.17 us -> 1.52 us  [body(): queries = new_query.reshape(seq_count, local_heads, HD)]
    pmax x1, blocking collectives: 11.7 us -> 12.8 us  [body(): maxima = lax.pmax(local_top, 'sp')]
    convert_element_type x1, other arithmetic: 2.53 us -> 1.64 us  [body(): normed = (as_float * lax.rsqrt(jnp.mean(as_float * as_float, axis=-1, kee...]
  transfers between devices with their start and end apart: 1 -> 3, of which waited for: 1 -> 3; matrix products, arithmetic and copies ran while one was open for 1% -> 5% of each run, Pallas kernels for 0% -> 0%
where the time goes in v1:
time: 79.8 us; the launch traced here: 79.3 us
  waiting for transfers between devices  39 us (49%)
  blocking collectives  21.3 us (27%)
  local copies, waits for them, and re-layouts  9.94 us (12%)
  other arithmetic  5.01 us (6%)
  matrix products  2.8 us (4%)
  between operations  0.8 us (1%)
    ppermute x3, waiting for transfers between devices, body(): lax.ppermute(ring[-1], 'tp', [(dev, (dev + 1) % 4) for dev in range(4)])  39 us
    pmax x1, blocking collectives, body(): maxima = lax.pmax(local_top, 'sp')  12.8 us
    psum x1, blocking collectives, body(): totals, weighted = lax.psum((totals, weighted), 'sp')  8.5 us
    unnamed x22, local copies, waits for them, and re-layouts  4.87 us
    dot_general x1, matrix products, body(): jnp.dot(rows, both_weights, preferred_element_type=jnp.float32)  2.35 us
    convert_element_type x1, other arithmetic, body(): normed = (as_float * lax.rsqrt(jnp.mean(as_float * as_float, axis=-1, kee...  1.64 us
  transfers between devices with their start and end apart: 3, of which 3 were waited for; matrix products, arithmetic and copies ran while one was open for 5% of the time, Pallas kernels for 0%

profile of v1, /device:TPU:0, one launch (start us, length us, event | category | flops | bytes accessed | tf_op | source)
XLA Modules:
  0.0 79.3 jit_solution(12259363461523371212)
XLA Ops:
  0.6 0.7 convert_element_type.35
  1.3 1.5 %fusion.4 = f32[2,64]{1,0:T(2,128)S(1)} fusion(bf16[2,64,4096]{2,1,0:T(8,128)(2,1)} %param.9), kind=kLoop, calls=%fused_computation.6 | loop fusion | flops 1572736 | bytes 1049088 | tf_op jit(solution)/shard_map/reduce_sum | solution.py:18
  2.9 1.6 %fusion.6 = bf16[2,64,4096]{2,1,0:T(8,128)(2,1)S(1)} fusion(bf16[2,64,4096]{2,1,0:T(8,128)(2,1)} %param.9, f32[4096]{0:T(1024)S(1)} %convert_element_type.35, f32[2,64]{1,0:T(2,128)S(1)} %add_rsqrt_fusion), kind=kLoop, calls=%fused_computation.8 | loop fusion | flops 2097152 | bytes 2114048 | tf_op jit(solution)/shard_map/convert_element_type | solution.py:20
  4.5 0.5 collective-permute-start
  5.1 14.4 %collective-permute-done = bf16[2,64,4096]{2,1,0:T(8,128)(2,1)S(1)} collective-permute-done((bf16[2,64,4096]{2,1,0:T(8,128)(2,1)S(1)}, bf16[2,64,4096]{2,1,0:T(8,128)(2,1)S(1)}, u32[]{:S(2)}, u32[]{:S(2)}) %collective-permute-start) | collective-permute-done | bytes 1048608 | tf_op jit(solution)/shard_map/ppermute | solution.py:26
  19.5 14.2 %collective-permute-done.1 = bf16[2,64,4096]{2,1,0:T(8,128)(2,1)S(1)} collective-permute-done((bf16[2,64,4096]{2,1,0:T(8,128)(2,1)S(1)}, bf16[2,64,4096]{2,1,0:T(8,128)(2,1)S(1)}, u32[]{:S(2)}, u32[]{:S(2)}) %collective-permute-start.1) | collective-permute-done | bytes 1048608 | tf_op jit(solution)/shard_map/ppermute | solution.py:26
  33.7 0.8 reshape.53
  34.4 0.8 reshape.44
  35.2 0.8 reshape.46
  36.0 0.8 reshape.47
  36.7 0.8 %slice_reduce_fusion = f32[2,4]{1,0:T(2,128)S(1)} fusion(f32[2,256,4]{1,2,0:T(4,128)} %param.13), kind=kLoop, calls=%fused_computation.26 | loop fusion | bytes 64 | tf_op jit(solution)/shard_map/slice | solution.py:53
  37.7 10.4 %collective-permute-done.2 = bf16[2,64,4096]{2,1,0:T(8,128)(2,1)} collective-permute-done((bf16[2,64,4096]{2,1,0:T(8,128)(2,1)S(1)}, bf16[2,64,4096]{2,1,0:T(8,128)(2,1)}, u32[]{:S(2)}, u32[]{:S(2)}) %collective-permute-start.2) | collective-permute-done | bytes 1048608 | tf_op jit(solution)/shard_map/ppermute | solution.py:26
  48.0 1.3 %constant_dynamic-update-slice_fusion.7 = bf16[2,512,4096]{2,1,0:T(8,128)(2,1)S(1)} fusion(bf16[2,64,4096]{2,1,0:T(8,128)(2,1)} %collective-permute-done.2), kind=kLoop, calls=%fused_computation.17 | loop fusion | bytes 2097152
  49.5 0.3 constant_dynamic-update-slice_fusion.4
  49.8 1.3 %constant_dynamic-update-slice_fusion.3 = bf16[2,512,4096]{2,1,0:T(8,128)(2,1)S(1)} fusion(bf16[2,512,4096]{2,1,0:T(8,128)(2,1)S(1)} %constant_dynamic-update-slice_fusion.4, bf16[2,64,4096]{2,1,0:T(8,128)(2,1)} %collective-permute-done.2), kind=kLoop, calls=%fused_computation.13 | loop fusion | bytes 2097152
  51.3 0.3 constant_dynamic-update-slice_fusion
  51.6 0.5 constant_dynamic-slice_fusion
  52.1 1.1 %copy-done.5 = bf16[4096,256]{1,0:T(8,128)(2,1)S(1)} copy-done((bf16[4096,256]{1,0:T(8,128)(2,1)S(1)}, bf16[4096,256]{1,0:T(8,128)(2,1)}, u32[]{:S(2)}) %copy-start.5) | copy-done | bytes 2097176
  53.2 0.6 copy-done.6
  53.8 2.3 %fusion.7 = bf16[512,512]{1,0:T(8,128)(2,1)S(1)} fusion(bf16[512,4096]{1,0:T(8,128)(2,1)S(1)} %bitcast.30, bf16[4096,256]{1,0:T(8,128)(2,1)S(1)} %copy-done.5, bf16[4096,256]{1,0:T(8,128)(2,1)S(1)} %copy-done.6), kind=kOutput, calls=%fused_computation.9 | convolution fusion | flops 2156134400 | bytes 8912896 | tf_op jit(solution)/shard_map/dot_general | solution.py:32
  56.8 12.8 %pmax.7 = f32[2,4]{1,0:T(2,128)S(1)} all-reduce(f32[2,4]{1,0:T(2,128)S(1)} %get-tuple-element.10), channel_id=1, replica_groups=mesh['gr'=2,'sp'=4,'tp'=4] {'sp'}, use_global_device_ids=true, to_apply=%region_3.4 | all-reduce | flops 8 | bytes 64 | tf_op jit(solution)/shard_map/pmax | solution.py:56
  69.7 0.3 fusion.10
  70.1 8.5 %all-reduce = (f32[2,4,64]{2,1,0:T(4,128)S(1)}, f32[2,4]{1,0:T(2,128)S(1)}) all-reduce(f32[2,4,64]{2,1,0:T(4,128)S(1)} %multiply_add_fusion, f32[2,4]{1,0:T(2,128)S(1)} %get-tuple-element.8), channel_id=1, replica_groups=mesh['gr'=2,'sp'=4,'tp'=4] {'sp'}, use_global_device_ids=true, to_apply=%region_4.5 | all-reduce | flops 520 | bytes 4160 | tf_op jit(solution)/shard_map/psum | solution.py:62
  78.7 0.7 convert_element_type.44
  (30 shorter events, 1.3 us)
Async XLA Ops:
  2.9 46.6 %copy-start = (bf16[2,64,4096]{2,1,0:T(8,128)(2,1)S(1)}, bf16[2,64,4096]{2,1,0:T(8,128)(2,1)}, u32[]{:S(2)}) copy-start(bf16[2,64,4096]{2,1,0:T(8,128)(2,1)} %param.9) | copy-start | bytes 3145732
  4.5 14.9 %collective-permute-start = (bf16[2,64,4096]{2,1,0:T(8,128)(2,1)S(1)}, bf16[2,64,4096]{2,1,0:T(8,128)(2,1)S(1)}, u32[]{:S(2)}, u32[]{:S(2)}) collective-permute-start(bf16[2,64,4096]{2,1,0:T(8,128)(2,1)S(1)} %fusion.6), channel_id=1, source_target_pairs={{0,1},{1,2},{2,3},{3,0},{4,5},{5,6},{6,7},{7,4},{8,9},{9,10},{10,1... | collective-permute-start | bytes 3145736 | tf_op jit(solution)/shard_map/ppermute | solution.py:26
  19.5 14.2 %collective-permute-start.1 = (bf16[2,64,4096]{2,1,0:T(8,128)(2,1)S(1)}, bf16[2,64,4096]{2,1,0:T(8,128)(2,1)S(1)}, u32[]{:S(2)}, u32[]{:S(2)}) collective-permute-start(bf16[2,64,4096]{2,1,0:T(8,128)(2,1)S(1)} %collective-permute-done), channel_id=1, source_target_pairs={{0,1},{1,2},{2,3},{3,0},{4,5},{5,6},{6,7},{7,4},{8,9},{9,10},{10,1... | collective-permute-start | bytes 3145736 | tf_op jit(solution)/shard_map/ppermute | solution.py:26
  33.7 14.3 %collective-permute-start.2 = (bf16[2,64,4096]{2,1,0:T(8,128)(2,1)S(1)}, bf16[2,64,4096]{2,1,0:T(8,128)(2,1)}, u32[]{:S(2)}, u32[]{:S(2)}) collective-permute-start(bf16[2,64,4096]{2,1,0:T(8,128)(2,1)S(1)} %collective-permute-done.1), channel_id=1, source_target_pairs={{0,1},{1,2},{2,3},{3,0},{4,5},{5,6},{6,7},{7,4},{8,9},{9,10},{10,1... | collective-permute-start | bytes 3145736 | tf_op jit(solution)/shard_map/ppermute | solution.py:26
  51.6 1.6 %copy-start.5 = (bf16[4096,256]{1,0:T(8,128)(2,1)S(1)}, bf16[4096,256]{1,0:T(8,128)(2,1)}, u32[]{:S(2)}) copy-start(bf16[4096,256]{1,0:T(8,128)(2,1)} %param.12) | copy-start | bytes 6291460
  51.6 2.2 %copy-start.6 = (bf16[4096,256]{1,0:T(8,128)(2,1)S(1)}, bf16[4096,256]{1,0:T(8,128)(2,1)}, u32[]{:S(2)}) copy-start(bf16[4096,256]{1,0:T(8,128)(2,1)} %param.11) | copy-start | bytes 6291460
  53.8 2.9 %copy-start.3 = (f32[2,256,4]{1,2,0:T(4,128)S(1)}, f32[2,256,4]{1,2,0:T(4,128)}, u32[]{:S(2)}) copy-start(f32[2,256,4]{1,2,0:T(4,128)} %param.13) | copy-start | bytes 24580
  53.8 3.0 %copy-start.4 = (f32[2,4]{1,0:T(2,128)S(1)}, f32[2,4]{1,0:T(2,128)}, u32[]{:S(2)}) copy-start(f32[2,4]{1,0:T(2,128)} %param.17) | copy-start | bytes 100
  56.2 23.1 %copy-start.1 = (bf16[2,256,256]{2,1,0:T(8,128)(2,1)}, bf16[2,256,256]{2,1,0:T(8,128)(2,1)S(1)}, u32[]{:S(2)}) copy-start(bf16[2,256,256]{2,1,0:T(8,128)(2,1)S(1)} %get-tuple-element.12) | copy-start | bytes 786436
  56.2 23.1 %copy-start.2 = (bf16[2,256,256]{2,1,0:T(8,128)(2,1)}, bf16[2,256,256]{2,1,0:T(8,128)(2,1)S(1)}, u32[]{:S(2)}) copy-start(bf16[2,256,256]{2,1,0:T(8,128)(2,1)S(1)} %get-tuple-element.13) | copy-start | bytes 786436
